TPU v7x, 32 devices: a whole 2x2x4 slice. The times are simulated.
32 devices in a mesh: grp: 2 (over y), ep: 8 (over z, x), tp: 2 (over core).
Axes of the slice: x: 2, y: 2, z: 4, core: 2. Of those that a mesh axis runs over, the one named last changes fastest.
Arguments:
- tokens: bfloat16 [2048, 2048], P(('grp', 'ep')), parts along dimension 0, may hold values from -6 to 6
- in_gain: float32 [2048], replicated, may hold values from 0.1 to 1.9
- routing: int32 [2048, 4], P(('grp', 'ep')), parts along dimension 0, may hold values from 0 to 15, as said below
- gate_prob: float32 [2048, 4], P(('grp', 'ep')), parts along dimension 0, may hold values from 0.05 to 1
- w_gate: bfloat16 [16, 2048, 512], P('ep', None, 'tp'), may hold values from -0.125 to 0.125
- w_up: bfloat16 [16, 2048, 512], P('ep', None, 'tp'), may hold values from -0.125 to 0.125
- w_down: bfloat16 [16, 512, 2048], P('ep', 'tp')
- out_gain: float32 [2048], P('tp'), may hold values from 0.1 to 1.9
Outputs:
- output: bfloat16 [2048, 2048], P(('grp', 'ep'), 'tp'), parts along dimension 0
There are 2 independent parts, one for each index of `grp`. A program takes and returns all parts, laid end to end along the dimension named above; an argument that names none is the same for every part. Nothing has to cross between parts.
Inputs may be any that keep to these rules, and one draw needn't show every extreme that they name: `routing`: each row names 4 different experts, all of one group (the same value of expert // 4). In the rows of one device no expert is named more than 64 times, and in every device's rows some expert is named exactly 64 times.
All inputs are finite; a program needn't handle non-finite values.
Results may differ from a plain program's by a relative error of at most 0.0077.
Values may be sent and summed in bfloat16 or wider, within the bound.
A program may use at most 64 MiB of HBM per device.

v0:
```python
import jax
import jax.numpy as jnp
from jax import lax
from jax.sharding import PartitionSpec as P

GROUPS = 4


EPS = 1e-06


def slot_ranks(flat_routes, expert_count):
    matches = (flat_routes[:, None] == jnp.arange(expert_count, dtype=jnp.int32)[None, :]).astype(
        jnp.int32
    )
    earlier = jnp.cumsum(matches, axis=0) - matches
    return jnp.sum(earlier * matches, axis=1)


def fill_rows(source, entries):
    filled = entries > 0
    return jnp.where(
        filled[:, None], source[jnp.maximum(entries - 1, 0)], jnp.zeros((), source.dtype)
    )


def body(tokens, in_gain, routing, gate_prob, w_gate, w_up, w_down, out_gain):
    ep_count = lax.axis_size("ep")
    local_experts = w_gate.shape[0]
    expert_count = local_experts * ep_count
    tok_dev, top_count = routing.shape
    model_width = tokens.shape[1]
    half_width = out_gain.shape[0]
    group_width = expert_count // GROUPS
    row_cap = max(2, tok_dev * top_count // (2 * group_width))
    floats = tokens.astype(jnp.float32)
    normed = (
        floats * lax.rsqrt(jnp.mean(floats * floats, axis=-1, keepdims=True) + EPS) * in_gain
    ).astype(jnp.bfloat16)
    flat_routes = routing.reshape(-1)
    slot_rank = slot_ranks(flat_routes, expert_count)
    slot_ids = flat_routes * row_cap + slot_rank
    token_ids = jnp.arange(tok_dev * top_count, dtype=jnp.int32) // top_count
    slot_table = jnp.zeros((expert_count * row_cap,), jnp.int32).at[slot_ids].set(token_ids + 1)
    own_columns = lax.dynamic_slice_in_dim(normed, lax.axis_index("tp") * half_width, half_width, 1)
    sendbuf = fill_rows(own_columns, slot_table).reshape(
        ep_count, local_experts, row_cap, half_width
    )
    arrived = lax.all_to_all(sendbuf, "ep", split_axis=0, concat_axis=0, tiled=True)
    arrived = lax.all_gather(arrived, "tp", axis=3, tiled=True)
    gate_act = jnp.einsum("secd,edf->secf", arrived, w_gate, preferred_element_type=jnp.float32)
    up_act = jnp.einsum("secd,edf->secf", arrived, w_up, preferred_element_type=jnp.float32)
    hidden = (jax.nn.silu(gate_act) * up_act).astype(jnp.bfloat16)
    partial_out = jnp.einsum("secf,efd->secd", hidden, w_down, preferred_element_type=jnp.float32)
    results = lax.psum_scatter(
        partial_out.astype(jnp.bfloat16), "tp", scatter_dimension=3, tiled=True
    )
    returned = lax.all_to_all(results, "ep", split_axis=0, concat_axis=0, tiled=True).reshape(
        expert_count * row_cap, half_width
    )
    picked = returned[slot_ids].astype(jnp.float32).reshape(tok_dev, top_count, half_width)
    mixed_rows = jnp.sum(picked * gate_prob[:, :, None], axis=1)
    squares = jnp.sum(mixed_rows * mixed_rows, axis=1)
    total_squares = lax.psum(squares, "tp")
    inv_rms = lax.rsqrt(total_squares / model_width + EPS)
    return (mixed_rows * inv_rms[:, None] * out_gain).astype(jnp.bfloat16)


def solution(mesh):
    placed = (
        P(("grp", "ep"), None),
        P(),
        P(("grp", "ep"), None),
        P(("grp", "ep"), None),
        P("ep", None, "tp"),
        P("ep", None, "tp"),
        P("ep", "tp", None),
        P("tp"),
    )
    return jax.shard_map(
        body, mesh=mesh, in_specs=placed, out_specs=P(("grp", "ep"), "tp"), check_vma=False
    )
```

profile of v0, /device:TPU:0, one launch (start us, length us, event | category | flops | bytes accessed | tf_op | source)
XLA Modules:
  0.0 192.8 jit_solution(13421549271625434358)
XLA Ops:
  6.6 1.3 convert_element_type.34
  7.8 1.2 multiply_reduce_fusion.1
  9.1 0.1 copy.19
  9.2 0.1 eq.29
  9.3 0.1 eq.25
  9.4 1.2 reduce-window.6
  10.6 0.2 slice_reduce_fusion
  10.9 0.1 copy.18
  11.0 0.1 mul.77
  11.1 0.1 fusion.24
  11.2 2.4 %scatter_custom_fusion = s32[1024]{0:T(1024)S(1)} fusion(s32[512]{0:T(512)S(1)} %bitcast.63, s32[512]{0:T(512)S(1)} %fusion.26, s32[]{:T(128)} %constant.19.clone.1), kind=kCustom, calls=%fused_computation.42 | custom fusion | bytes 4100 | tf_op jit(solution)/shard_map/scatter | solution.py:44
  13.7 0.1 broadcast_in_dim.16
  13.8 0.1 fusion.20
  13.9 5.4 %gather_fusion = bf16[1024,1024]{1,0:T(8,128)(2,1)} fusion(bf16[128,1024]{1,0:T(8,128)(2,1)S(1)} %fusion.20, s32[1024]{0:T(1024)S(1)} %maximum_clamp_fusion), kind=kCustom, calls=%fused_computation | custom fusion | bytes 4198400 | tf_op jit(solution)/shard_map/gather | solution.py:23
  19.3 1.8 broadcast_select_fusion
  21.1 55.3 %all_to_all.10 = bf16[8,2,64,1024]{3,2,1,0:T(8,128)(2,1)S(1)} all-to-all(bf16[8,2,64,1024]{3,2,1,0:T(8,128)(2,1)S(1)} %broadcast_select_fusion), channel_id=1, replica_groups=mesh['grp'=2,'ep'=8,'tp'=2] {'ep'}, dimensions={0} | all-to-all | bytes 4194304 | tf_op jit(solution)/shard_map/all_to_all | solution.py:49
  76.4 1.5 copy.22
  78.0 0.0 reduce-scatter.2.cloned.1.call-start
  78.0 12.8 %all-gather.2.cloned.1.call-done = bf16[8,2,64,2048]{3,2,0,1:T(8,128)(2,1)} async-done(((bf16[8,2,64,1024]{3,2,0,1:T(8,128)(2,1)}), bf16[8,2,64,2048]{3,2,0,1:T(8,128)(2,1)}) %all-gather.2.cloned.1.call-update) | async-done | bytes 4194320 | tf_op jit(solution)/shard_map/all_gather | solution.py:50
  90.8 4.1 %fusion.5 = f32[8,2,64,256]{3,2,0,1:T(8,128)S(1)} fusion(bf16[8,2,64,2048]{3,2,0,1:T(8,128)(2,1)} %all-gather.2.cloned.1.call-done, bf16[2,2048,256]{2,1,0:T(8,128)(2,1)} %param.12), kind=kOutput, calls=%fused_computation.11 | convolution fusion | flops 1073741824 | bytes 7340032 | tf_op jit(solution)/shard_map/secd,edf->secf/dot_general | solution.py:51
  94.9 7.3 %convert_bitcast_fusion = bf16[8,2,64,2048]{3,2,0,1:T(8,128)(2,1)} fusion(bf16[2,256,2048]{2,1,0:T(8,128)(2,1)S(1)} %copy-done, bf16[8,2,64,2048]{3,2,0,1:T(8,128)(2,1)} %all-gather.2.cloned.1.call-done, bf16[2,2048,256]{2,1,0:T(8,128)(2,1)} %param.13, f32[8,2,64,256]{3,2,0,1:T(8,128)S(1)} %fusion.5), kind=kOutput, calls=%fused_computation.3 | convolution fusion | flops 2151153664 | bytes 13631488 | tf_op jit(solution)/shard_map/secf,efd->secd/dot_general | solution.py:54
  102.3 13.2 %reduce-scatter.2.cloned.1.call-done = bf16[8,2,64,1024]{3,2,0,1:T(8,128)(2,1)} async-done(((bf16[8,2,64,2048]{3,2,0,1:T(8,128)(2,1)}), bf16[8,2,64,1024]{3,2,0,1:T(8,128)(2,1)}) %reduce-scatter.2.cloned.1.call-update) | async-done | bytes 2097168 | tf_op jit(solution)/shard_map/reduce_scatter | solution.py:55
  115.5 3.1 %copy.23 = bf16[8,2,64,1024]{3,2,1,0:T(8,128)(2,1)} copy(bf16[8,2,64,1024]{3,2,0,1:T(8,128)(2,1)} %reduce-scatter.2.cloned.1.call-done) | data formatting | bytes 4194304 | tf_op jit(solution)/shard_map/reduce_scatter | solution.py:55
  118.6 6.0 %all-to-all-start.1 = ((bf16[8,2,64,1024]{3,2,1,0:T(8,128)(2,1)}), bf16[8,2,64,1024]{3,2,1,0:T(8,128)(2,1)}, u32[]{:S(2)}, u32[]{:S(2)}) async-start(bf16[8,2,64,1024]{3,2,1,0:T(8,128)(2,1)} %copy.23), calls=%async_computation.2 | async-start | bytes 4194304 | tf_op jit(solution)/shard_map/all_to_all | solution.py:58
  124.6 0.1 copy.24
  124.7 48.5 %all-to-all-done.1 = bf16[8,2,64,1024]{3,2,1,0:T(8,128)(2,1)} async-done(((bf16[8,2,64,1024]{3,2,1,0:T(8,128)(2,1)}), bf16[8,2,64,1024]{3,2,1,0:T(8,128)(2,1)}, u32[]{:S(2)}, u32[]{:S(2)}) %all-to-all-start.1) | async-done | bytes 2097184 | tf_op jit(solution)/shard_map/all_to_all | solution.py:58
  173.3 4.6 %gather_fusion.1 = bf16[512,1024]{1,0:T(8,128)(2,1)S(1)} fusion(bf16[1024,1024]{1,0:T(8,128)(2,1)} %bitcast.13, s32[1024]{0:T(1024)S(1)} %pad_clamp_fusion), kind=kCustom, calls=%fused_computation.1 | custom fusion | bytes 2099200 | tf_op jit(solution)/shard_map/gather | solution.py:61
  177.9 1.7 reshape.75
  179.6 3.0 %multiply_reduce_fusion = f32[128,1024]{1,0:T(8,128)S(1)} fusion(f32[128,4,1024]{2,1,0:T(4,128)} %reshape.75, f32[128,4]{1,0:T(8,128)S(1)} %copy.24), kind=kLoop, calls=%fused_computation.9 | loop fusion | flops 917504 | bytes 2623488 | tf_op jit(solution)/shard_map/reduce_sum | solution.py:62
  182.6 0.1 multiply_reduce_fusion.2
  182.7 2.5 %psum.7 = f32[128]{0:T(128)S(1)} all-reduce(f32[128]{0:T(128)S(1)} %multiply_reduce_fusion.2), channel_id=1, replica_groups=mesh['grp'=2,'ep'=8,'tp'=2] {'tp'}, use_global_device_ids=true, to_apply=%region_8.9 | all-reduce | flops 128 | bytes 1024 | tf_op jit(solution)/shard_map/psum | solution.py:64
  185.2 0.8 multiply_convert_fusion
  (25 shorter events, 0.2 us)
Async XLA Ops:
  6.5 88.4 %copy-start = (bf16[2,256,2048]{2,1,0:T(8,128)(2,1)S(1)}, bf16[2,256,2048]{2,1,0:T(8,128)(2,1)}, u32[]{:S(2)}) copy-start(bf16[2,256,2048]{2,1,0:T(8,128)(2,1)} %param.14) | copy-start | bytes 6291460
  6.5 2.5 %copy-start.1 = (s32[128,4]{0,1:T(4,128)S(1)}, s32[128,4]{0,1:T(4,128)}, u32[]{:S(2)}) copy-start(s32[128,4]{0,1:T(4,128)} %param.10) | copy-start | bytes 6148
  6.5 7.2 %copy-start.4 = (f32[2048]{0:T(1024)S(1)}, f32[2048]{0:T(1024)}, u32[]{:S(2)}) copy-start(f32[2048]{0:T(1024)} %param.9) | copy-start | bytes 24580
  6.5 84.3 %all-gather.2.cloned.1.call-start = ((), (), s32[]{:S(2)}) async-start(), calls=%async_computation.3 | async-start | bytes 6291456 | tf_op jit(solution)/shard_map/all_gather | solution.py:50
  78.0 37.5 %reduce-scatter.2.cloned.1.call-start = ((), (), s32[]{:S(2)}) async-start(), calls=%async_computation.4 | async-start | bytes 6291456 | tf_op jit(solution)/shard_map/reduce_scatter | solution.py:55
  118.6 6.0 %copy-start.3 = (f32[128,4]{0,1:T(4,128)S(1)}, f32[128,4]{0,1:T(4,128)}, u32[]{:S(2)}) copy-start(f32[128,4]{0,1:T(4,128)} %param.11) | copy-start | bytes 6148
  118.6 54.7 %all-to-all-start.1 = ((bf16[8,2,64,1024]{3,2,1,0:T(8,128)(2,1)}), bf16[8,2,64,1024]{3,2,1,0:T(8,128)(2,1)}, u32[]{:S(2)}, u32[]{:S(2)}) async-start(bf16[8,2,64,1024]{3,2,1,0:T(8,128)(2,1)} %copy.23), calls=%async_computation.2 | async-start | bytes 4194304 | tf_op jit(solution)/shard_map/all_to_all | solution.py:58
  179.6 5.6 %copy-start.2 = (f32[1024]{0:T(1024)S(1)}, f32[1024]{0:T(1024)}, u32[]{:S(2)}) copy-start(f32[1024]{0:T(1024)} %param.15) | copy-start | bytes 12292
Sparse Core Ops, SparseCore 0:
  78.1 12.6 all-gather.1
  102.4 13.0 reduce-scatter.1
where the time goes:
time: 193 us
  waiting for transfers between devices  74.6 us (39%)
  blocking collectives  57.8 us (30%)
  local copies, waits for them, and re-layouts  19.8 us (10%)
  between operations  13.6 us (7%)
  matrix products  11.4 us (6%)
  other arithmetic  9.68 us (5%)
  starting transfers between devices  6.06 us (3%)
    all_to_all x1, blocking collectives, body(): lax.all_to_all(sendbuf, 'ep', split_axis=0, concat_axis=0, tiled=True)  55.3 us
    all_to_all x1, waiting for transfers between devices, body(): lax.all_to_all(results, 'ep', split_axis=0, concat_axis=0, tiled=True)  48.5 us
    reduce_scatter x1, waiting for transfers between devices, body(): lax.psum_scatter(partial_out.astype(jnp.bfloat16), 'tp', scatter_dimensio...  13.2 us
    all_gather x1, waiting for transfers between devices, body(): arrived = lax.all_gather(arrived, 'tp', axis=3, tiled=True)  12.8 us
    dot_general x1, matrix products, body(): jnp.einsum('secf,efd->secd', hidden, w_down, preferred_element_type=jnp.f...  7.3 us
    all_to_all x1, starting transfers between devices, body(): lax.all_to_all(results, 'ep', split_axis=0, concat_axis=0, tiled=True)  6.02 us
    gather x1, local copies, waits for them, and re-layouts, fill_rows(): source[jnp.maximum(entries - 1, 0)]  5.36 us
    gather x1, local copies, waits for them, and re-layouts, body(): returned[slot_ids].astype(jnp.float32)  4.59 us
  transfers between devices with their start and end apart: 3, of which 3 were waited for; matrix products, arithmetic and copies ran while one was open for 0% of the time, Pallas kernels for 0%

commit v1 on v0

v1 whole, which is shorter than its diff:
```python
import functools

import jax
import jax.numpy as jnp
from jax import lax
from jax.experimental import pallas as pl
from jax.experimental.pallas import tpu as pltpu
from jax.sharding import PartitionSpec as P

GROUPS = 4
EPS = 1e-06
MESH = pl.DeviceIdType.MESH
F32 = jnp.float32
BF16 = jnp.bfloat16


def loop(low, high, step):
    if high - low <= 8:
        for i in range(low, high):
            step(i)
    else:
        lax.fori_loop(low, high, lambda i, carry: (step(i), carry)[1], 0)


def kernel(
    group_count, span, rows,
    routes_ref, probs_ref, in_gain_ref, out_gain_ref, tokens_ref, gate_hbm, up_hbm, down_hbm,
    out_ref,
    sendz, gathered, unpack, gate_send, gate_recv, w_gate, w_up, w_down, hidden,
    kept, tp_send, tp_recv, own_sum, grp_recv, home_send, home_recv, sq_send, sq_recv,
    w_sem, gate_ss, gate_rs, z_ss, z_rs, x_ss, x_rs, t_ss, t_rs, p_ss, p_rs, r_ss, r_rs, h_ss, h_rs, q_ss, q_rs,
):
    Q, S, R = group_count, span, rows
    N = Q * S
    top, tok = routes_ref.shape
    width = tokens_ref.shape[1]
    H = out_ref.shape[1]
    L, _, F = gate_hbm.shape
    group_width = S * L
    gate_rows, lanes = gate_send.shape[1:]
    me = lax.axis_index("ep")
    c = lax.axis_index("tp")
    q, s = me // S, lax.rem(me, S)
    order = [0] + sorted(range(1, Q), key=lambda d: -min(d, Q - d))

    def at(ep, tp=None):
        return {"ep": ep, "tp": c if tp is None else tp}

    def remote(src, dst, ss, rs, dev):
        return pltpu.make_async_remote_copy(
            src_ref=src, dst_ref=dst, send_sem=ss, recv_sem=rs, device_id=dev, device_id_type=MESH
        )

    barrier = pltpu.get_barrier_semaphore()
    loop(1, N, lambda p: pl.semaphore_signal(
        barrier, inc=1, device_id=at(lax.rem(me + p, N)), device_id_type=MESH))
    pl.semaphore_signal(barrier, inc=1, device_id=at(me, 1 - c), device_id_type=MESH)

    weights = []
    for n, (src, dst) in enumerate(((gate_hbm, w_gate), (up_hbm, w_up), (down_hbm, w_down))):
        for e in range(L):
            weights.append(pltpu.make_async_copy(src.at[e], dst.at[e], w_sem.at[n, e]))
    for copy in weights:
        copy.start()

    floats = tokens_ref[...].astype(F32)
    inv = lax.rsqrt(jnp.mean(floats * floats, axis=-1, keepdims=True) + EPS)
    own_cols = pl.ds(pl.multiple_of(c * H, H), H)
    other_cols = pl.ds(pl.multiple_of((1 - c) * H, H), H)
    normed = (tokens_ref[:, own_cols].astype(F32) * inv * in_gain_ref[:, own_cols]).astype(BF16)
    first = routes_ref[0:1, :]
    groups = lax.broadcasted_iota(jnp.int32, (16, tok), 0)
    member = (first >= groups * group_width) & (first < (groups + 1) * group_width)
    earlier = lax.broadcasted_iota(jnp.int32, (tok, tok), 0) < lax.broadcasted_iota(jnp.int32, (tok, tok), 1)
    rank = jnp.dot(
        jnp.where(member, 1.0, 0.0).astype(BF16), jnp.where(earlier, 1.0, 0.0).astype(BF16),
        preferred_element_type=F32,
    ).astype(jnp.int32)
    slots = lax.broadcasted_iota(jnp.int32, (lanes, tok), 0)
    picks = []
    for g in range(Q):
        inside = (first >= g * group_width) & (first < (g + 1) * group_width)
        picks.append(jnp.where((rank[g:g + 1, :] == slots) & inside, 1.0, 0.0))
        sendz[g] = jnp.dot(
            picks[g][:R].astype(BF16), normed, preferred_element_type=F32
        ).astype(BF16)

    gathered[q, s, c] = sendz[q]
    pl.semaphore_wait(barrier, N)

    def z_copy(d):
        to = lax.rem(q + d, Q)
        return remote(sendz.at[to], gathered.at[q, s, c], z_ss.at[d], z_rs.at[d], at(to * S + s))

    def source(d):
        return lax.rem(q + Q - d, Q)

    def x_copy(d, e):
        block = gathered.at[source(d), s, c]
        return remote(block, block, x_ss.at[d, e], x_rs.at[d, e], at(q * S + lax.rem(s + e, S)))

    def t_copy(d, e):
        block = gathered.at[source(d), lax.rem(s + S - e, S), c]
        return remote(block, block, t_ss.at[d, e], t_rs.at[d, e], at(me, 1 - c))

    def gate_copy(p):
        to = lax.rem(me + p, N)
        return remote(gate_send.at[to // S], gate_recv.at[me], gate_ss.at[p], gate_rs.at[p], at(to))

    def p_copy(d):
        return remote(tp_send.at[d], tp_recv.at[d], p_ss.at[d], p_rs.at[d], at(me, 1 - c))

    def r_copy(d, e):
        to = lax.rem(s + e, S)
        return remote(tp_send.at[d, to], grp_recv.at[d, e], r_ss.at[d, e], r_rs.at[d, e], at(q * S + to))

    def h_copy(d):
        return remote(home_send.at[d], home_recv.at[q], h_ss.at[d], h_rs.at[d], at(source(d) * S + s))

    def forward(d):
        loop(1, S, lambda e: x_copy(d, e).start())
        t_copy(d, 0).start()

    for d in order[1:]:
        z_copy(d).start()
    forward(0)

    for g in range(Q):
        ids = g * group_width + lax.broadcasted_iota(jnp.int32, (gate_rows, tok), 0)
        dense = jnp.zeros((gate_rows, tok), F32)
        for k in range(top):
            dense += jnp.where(routes_ref[k:k + 1, :] == ids, probs_ref[k:k + 1, :], 0.0)
        gate_send[g] = lax.dot_general(
            dense, picks[g], (((1,), (1,)), ((), ())),
            precision=lax.Precision.HIGHEST, preferred_element_type=F32,
        )
    gate_recv[me] = gate_send[q]
    loop(1, N, lambda p: gate_copy(p).start())
    unpack[...] = jnp.concatenate([pick[:R] for pick in picks], axis=0).T.astype(BF16)

    def stage_a(d):
        z_copy(d).wait_recv()
        forward(d)

    def stage_b(d):
        def one(e):
            x_copy(d, e).wait_recv()
            t_copy(d, e).start()
        loop(1, S, one)

    pair = 2 if S % 2 == 0 else 1

    def stage_c(d):
        loop(0, S, lambda e: t_copy(d, e).wait_recv())
        src = source(d)
        diagonal = (
            lax.broadcasted_iota(jnp.int32, (R, lanes), 0) == lax.broadcasted_iota(jnp.int32, (R, lanes), 1)
        )

        def some(n):
            base = n * pair
            low = gathered[src, pl.ds(base, pair), 0].reshape(pair * R, H)
            high = gathered[src, pl.ds(base, pair), 1].reshape(pair * R, H)
            for j in range(L):
                gate = jnp.dot(low, w_gate[j, :H], preferred_element_type=F32)
                gate += jnp.dot(high, w_gate[j, H:], preferred_element_type=F32)
                up = jnp.dot(low, w_up[j, :H], preferred_element_type=F32)
                up += jnp.dot(high, w_up[j, H:], preferred_element_type=F32)
                scales = []
                for b in range(pair):
                    line = gate_recv[src * S + base + b, pl.ds(s * L + j, 1), :]
                    scales.append(jnp.sum(jnp.where(diagonal, line, 0.0), axis=1, keepdims=True))
                scale = jnp.concatenate(scales, axis=0)
                act = gate / (1.0 + jnp.exp(-gate)) * up
                hidden[:, j * F:(j + 1) * F] = (act * scale).astype(BF16)
            other = jnp.zeros((pair * R, H), F32)
            mine = jnp.zeros((pair * R, H), F32)
            for j in range(L):
                other += jnp.dot(hidden[:, j * F:(j + 1) * F], w_down[j, :, other_cols], preferred_element_type=F32)
            tp_send[d, pl.ds(base, pair)] = other.astype(BF16).reshape(pair, R, H)
            for j in range(L):
                mine += jnp.dot(hidden[:, j * F:(j + 1) * F], w_down[j, :, own_cols], preferred_element_type=F32)
            kept[pl.ds(base, pair)] = mine.reshape(pair, R, H)

        if S == pair:
            some(0)
        else:
            lax.fori_loop(0, S // pair, lambda n, carry: (some(n), carry)[1], 0)
        p_copy(d).start()

    def stage_e(d):
        p_copy(d).wait()
        def one(e):
            to = lax.rem(s + e, S)
            tp_send[d, to] = (kept[to] + tp_recv[d, to].astype(F32)).astype(BF16)
            r_copy(d, e).start()
        loop(1, S, one)
        own_sum[...] = kept[s] + tp_recv[d, s].astype(F32)

    def stage_f(d):
        def one(e):
            r_copy(d, e).wait_recv()
            own_sum[...] += grp_recv[d, e].astype(F32)
        loop(1, S, one)
        if d == 0:
            home_recv[q] = own_sum[...].astype(BF16)
        else:
            home_send[d] = own_sum[...].astype(BF16)
            h_copy(d).start()

    stage_b(0)
    for i in range(Q):
        if i + 1 < Q:
            stage_a(order[i + 1])
        if i == 0:
            loop(1, N, lambda p: gate_copy(p).wait_recv())
            for copy in weights:
                copy.wait()
        if i >= 1:
            if i >= 2:
                stage_f(order[i - 2])
            stage_e(order[i - 1])
        stage_c(order[i])
        if i + 1 < Q:
            stage_b(order[i + 1])
    if Q >= 2:
        stage_f(order[Q - 2])
    stage_e(order[Q - 1])
    stage_f(order[Q - 1])

    for d in order[1:]:
        h_copy(d).wait_recv()
    mixed = jnp.dot(unpack[...], home_recv[...].reshape(Q * R, H), preferred_element_type=F32)
    squares = jnp.sum(mixed * mixed, axis=1, keepdims=True)
    sq_send[...] = jnp.broadcast_to(squares, sq_send.shape)
    sq_copy = remote(sq_send, sq_recv, q_ss, q_rs, at(me, 1 - c))
    sq_copy.start()
    for d in range(1, Q):
        z_copy(d).wait_send()
        h_copy(d).wait_send()
    for d in range(Q):
        def sent(e):
            x_copy(d, e).wait_send()
            r_copy(d, e).wait_send()
        loop(1, S, sent)
        loop(0, S, lambda e: t_copy(d, e).wait_send())
    loop(1, N, lambda p: gate_copy(p).wait_send())
    sq_copy.wait()
    total = squares + sq_recv[:, 0:1]
    out_ref[...] = (mixed * lax.rsqrt(total / width + EPS) * out_gain_ref[...]).astype(BF16)


def body(tokens, in_gain, routing, gate_prob, w_gate, w_up, w_down, out_gain):
    N = lax.axis_size("ep")
    L, D, F = w_gate.shape
    tok, top = routing.shape
    H = out_gain.shape[0]
    group_width = L * N // GROUPS
    cap = max(2, tok * top // (2 * group_width))
    R = min(tok, group_width * cap // top)
    R = -(-R // 16) * 16
    Q, S = GROUPS, N // GROUPS
    lanes = -(-R // 128) * 128
    gate_rows = -(-group_width // 8) * 8
    pair = 2 if S % 2 == 0 else 1
    vmem = pl.BlockSpec(memory_space=pltpu.VMEM)
    hbm = pl.BlockSpec(memory_space=pl.ANY)
    dma = pltpu.SemaphoreType.DMA
    return pl.pallas_call(
        functools.partial(kernel, Q, S, R),
        out_shape=jax.ShapeDtypeStruct((tok, H), BF16),
        in_specs=[vmem] * 5 + [hbm] * 3,
        out_specs=vmem,
        scratch_shapes=[
            pltpu.VMEM((Q, R, H), BF16),
            pltpu.VMEM((Q, S, 2, R, H), BF16),
            pltpu.VMEM((tok, Q * R), BF16),
            pltpu.VMEM((Q, gate_rows, lanes), F32),
            pltpu.VMEM((N, gate_rows, lanes), F32),
            pltpu.VMEM((L, D, F), BF16),
            pltpu.VMEM((L, D, F), BF16),
            pltpu.VMEM((L, F, D), BF16),
            pltpu.VMEM((pair * R, L * F), BF16),
            pltpu.VMEM((S, R, H), F32),
            pltpu.VMEM((Q, S, R, H), BF16),
            pltpu.VMEM((Q, S, R, H), BF16),
            pltpu.VMEM((R, H), F32),
            pltpu.VMEM((Q, S, R, H), BF16),
            pltpu.VMEM((Q, R, H), BF16),
            pltpu.VMEM((Q, R, H), BF16),
            pltpu.VMEM((tok, 128), F32),
            pltpu.VMEM((tok, 128), F32),
            dma((3, L)), dma((N,)), dma((N,)), dma((Q,)), dma((Q,)),
            dma((Q, S)), dma((Q, S)), dma((Q, S)), dma((Q, S)),
            dma((Q,)), dma((Q,)), dma((Q, S)), dma((Q, S)), dma((Q,)), dma((Q,)),
            dma, dma,
        ],
        compiler_params=pltpu.CompilerParams(
            collective_id=0, has_side_effects=True, vmem_limit_bytes=64 * 1000 * 1000
        ),
    )(routing.T, gate_prob.T, in_gain.reshape(1, D), out_gain.reshape(1, H), tokens, w_gate, w_up, w_down)


def solution(mesh):
    placed = (
        P(("grp", "ep"), None),
        P(),
        P(("grp", "ep"), None),
        P(("grp", "ep"), None),
        P("ep", None, "tp"),
        P("ep", None, "tp"),
        P("ep", "tp", None),
        P("tp"),
    )
    return jax.shard_map(
        body, mesh=mesh, in_specs=placed, out_specs=P(("grp", "ep"), "tp"), check_vma=False
    )
```

time: 193 us -> 52.4 us (0.27)
  waiting for transfers between devices: 74.6 us -> 0 us
  blocking collectives: 57.8 us -> 0 us
  Pallas kernels: 0 us -> 50.5 us
  local copies, waits for them, and re-layouts: 19.8 us -> 1.67 us
  between operations: 13.6 us -> 0.01 us
  matrix products: 11.4 us -> 0 us
  other arithmetic: 9.68 us -> 0 us
  starting transfers between devices: 6.06 us -> 0 us
    all_to_all x1 -> x0, blocking collectives: 55.3 us -> none  [body(): lax.all_to_all(sendbuf, 'ep', split_axis=0, concat_axis=0, tiled=True)]
    pallas_call x0 -> x1, Pallas kernels: none -> 50.5 us  [body(): pl.pallas_call(functools.partial(kernel, Q, S, R), out_shape=jax.ShapeDty...]
    all_to_all x1 -> x0, waiting for transfers between devices: 48.5 us -> none  [body(): lax.all_to_all(results, 'ep', split_axis=0, concat_axis=0, tiled=True)]
    reduce_scatter x1 -> x0, waiting for transfers between devices: 13.2 us -> none  [body(): lax.psum_scatter(partial_out.astype(jnp.bfloat16), 'tp', scatter_dimensio...]
    all_gather x1 -> x0, waiting for transfers between devices: 12.8 us -> none  [body(): arrived = lax.all_gather(arrived, 'tp', axis=3, tiled=True)]
    dot_general x2 -> x0, matrix products: 11.4 us -> none  [the longest x1 7.3 us: body(): jnp.einsum('secf,efd->secd', hidden, w_down, preferred_element_type=jnp.f...]
    gather x2 -> x0, local copies, waits for them, and re-layouts: 9.95 us -> none  [the longest x1 5.36 us: fill_rows(): source[jnp.maximum(entries - 1, 0)]]
    all_to_all x1 -> x0, starting transfers between devices: 6.02 us -> none  [body(): lax.all_to_all(results, 'ep', split_axis=0, concat_axis=0, tiled=True)]
  transfers between devices with their start and end apart: 3 -> 0, of which waited for: 3 -> 0; matrix products, arithmetic and copies ran while one was open for 0% -> 0% of each run, Pallas kernels for 0% -> 0%
where the time goes in v1:
time: 52.4 us; the launch traced here: 52.2 us
  Pallas kernels  50.5 us (96%)
  local copies, waits for them, and re-layouts  1.67 us (3%)
    pallas_call x1, Pallas kernels, body(): pl.pallas_call(functools.partial(kernel, Q, S, R), out_shape=jax.ShapeDty...  50.5 us
    unnamed x1, local copies, waits for them, and re-layouts  1.67 us

profile of v1, /device:TPU:0, one launch (start us, length us, event | category | flops | bytes accessed | tf_op | source)
XLA Modules:
  0.0 52.2 jit_solution(15965704761108413742)
XLA Ops:
  0.0 50.5 %shard_map.82 = bf16[128,1024]{1,0:T(8,128)(2,1)} custom-call(s32[4,128]{1,0:T(4,128)} %bitcast.6, f32[4,128]{1,0:T(4,128)} %bitcast.7, f32[1,2048]{1,0:T(1,128)} %bitcast.4, f32[1,1024]{1,0:T(1,128)} %bitcast.5, bf16[128,2048]{1,0:T(8,128)(2,1)} %tokens_ref.1, bf16[2,2048,256]{2,1,0:T(8,128)(2,1)} %gate_hbm.1, bf16[2,2048,256]{2,1,0:T(8,128)(2,1)} %up_hbm.1, ...), custom_call_target="tpu_custom_call" | custom-call | tf_op jit(solution)/shard_map/pallas_call | solution.py:269
  50.6 1.7 %copy.10 = bf16[128,1024]{1,0:T(8,128)(2,1)} copy(bf16[128,1024]{1,0:T(8,128)(2,1)} %shard_map.82) | data formatting | bytes 524288

commit v2 on v1

--- a/solution.py
+++ b/solution.py
@@ -9,6 +9,7 @@
 
 GROUPS = 4
 EPS = 1e-06
+CHUNKS = 2
 MESH = pl.DeviceIdType.MESH
 F32 = jnp.float32
 BF16 = jnp.bfloat16
@@ -24,14 +25,16 @@
 
 def kernel(
     group_count, span, rows,
-    routes_ref, probs_ref, in_gain_ref, out_gain_ref, tokens_ref, gate_hbm, up_hbm, down_hbm,
+    routes_ref, probs_ref, in_gain_ref, out_gain_ref, tokens_hbm, gate_hbm, up_hbm, down_hbm,
     out_ref,
-    sendz, gathered, unpack, gate_send, gate_recv, w_gate, w_up, w_down, hidden,
+    tokens_ref, sendz, gathered, unpack, gate_send, gate_recv, w_gate, w_up, w_down, hidden,
     kept, tp_send, tp_recv, own_sum, grp_recv, home_send, home_recv, sq_send, sq_recv,
-    w_sem, gate_ss, gate_rs, z_ss, z_rs, x_ss, x_rs, t_ss, t_rs, p_ss, p_rs, r_ss, r_rs, h_ss, h_rs, q_ss, q_rs,
+    tok_sem, w_sem, gate_ss, gate_rs, z_ss, z_rs, x_ss, x_rs, t_ss, t_rs, p_ss, p_rs, r_ss, r_rs, h_ss, h_rs, q_ss, q_rs,
 ):
     Q, S, R = group_count, span, rows
     N = Q * S
+    K = CHUNKS
+    RC = R // K
     top, tok = routes_ref.shape
     width = tokens_ref.shape[1]
     H = out_ref.shape[1]
@@ -51,6 +54,9 @@
             src_ref=src, dst_ref=dst, send_sem=ss, recv_sem=rs, device_id=dev, device_id_type=MESH
         )
 
+    tok_copy = pltpu.make_async_copy(tokens_hbm, tokens_ref, tok_sem)
+    tok_copy.start()
+
     barrier = pltpu.get_barrier_semaphore()
     loop(1, N, lambda p: pl.semaphore_signal(
         barrier, inc=1, device_id=at(lax.rem(me + p, N)), device_id_type=MESH))
@@ -63,11 +69,6 @@
     for copy in weights:
         copy.start()
 
-    floats = tokens_ref[...].astype(F32)
-    inv = lax.rsqrt(jnp.mean(floats * floats, axis=-1, keepdims=True) + EPS)
-    own_cols = pl.ds(pl.multiple_of(c * H, H), H)
-    other_cols = pl.ds(pl.multiple_of((1 - c) * H, H), H)
-    normed = (tokens_ref[:, own_cols].astype(F32) * inv * in_gain_ref[:, own_cols]).astype(BF16)
     first = routes_ref[0:1, :]
     groups = lax.broadcasted_iota(jnp.int32, (16, tok), 0)
     member = (first >= groups * group_width) & (first < (groups + 1) * group_width)
@@ -81,6 +82,14 @@
     for g in range(Q):
         inside = (first >= g * group_width) & (first < (g + 1) * group_width)
         picks.append(jnp.where((rank[g:g + 1, :] == slots) & inside, 1.0, 0.0))
+
+    tok_copy.wait()
+    floats = tokens_ref[...].astype(F32)
+    inv = lax.rsqrt(jnp.mean(floats * floats, axis=-1, keepdims=True) + EPS)
+    own_cols = pl.ds(pl.multiple_of(c * H, H), H)
+    other_cols = pl.ds(pl.multiple_of((1 - c) * H, H), H)
+    normed = (tokens_ref[:, own_cols].astype(F32) * inv * in_gain_ref[:, own_cols]).astype(BF16)
+    for g in range(Q):
         sendz[g] = jnp.dot(
             picks[g][:R].astype(BF16), normed, preferred_element_type=F32
         ).astype(BF16)
@@ -88,42 +97,54 @@
     gathered[q, s, c] = sendz[q]
     pl.semaphore_wait(barrier, N)
 
-    def z_copy(d):
+    def z_copy(d, k):
         to = lax.rem(q + d, Q)
-        return remote(sendz.at[to], gathered.at[q, s, c], z_ss.at[d], z_rs.at[d], at(to * S + s))
+        part = pl.ds(k * RC, RC)
+        return remote(
+            sendz.at[to, part], gathered.at[q, s, c, part], z_ss.at[d, k], z_rs.at[d, k], at(to * S + s)
+        )
 
     def source(d):
         return lax.rem(q + Q - d, Q)
 
-    def x_copy(d, e):
-        block = gathered.at[source(d), s, c]
-        return remote(block, block, x_ss.at[d, e], x_rs.at[d, e], at(q * S + lax.rem(s + e, S)))
-
-    def t_copy(d, e):
-        block = gathered.at[source(d), lax.rem(s + S - e, S), c]
-        return remote(block, block, t_ss.at[d, e], t_rs.at[d, e], at(me, 1 - c))
-
-    def gate_copy(p):
-        to = lax.rem(me + p, N)
-        return remote(gate_send.at[to // S], gate_recv.at[me], gate_ss.at[p], gate_rs.at[p], at(to))
+    def x_copy(d, e, k):
+        block = gathered.at[source(d), s, c, pl.ds(k * RC, RC)]
+        return remote(block, block, x_ss.at[d, e, k], x_rs.at[d, e, k], at(q * S + lax.rem(s + e, S)))
+
+    def t_copy(d, e, k):
+        block = gathered.at[source(d), lax.rem(s + S - e, S), c, pl.ds(k * RC, RC)]
+        return remote(block, block, t_ss.at[d, e, k], t_rs.at[d, e, k], at(me, 1 - c))
+
+    def gate_copy(d, e):
+        to_q, to_s = lax.rem(q + d, Q), lax.rem(s + e, S)
+        return remote(
+            gate_send.at[to_q], gate_recv.at[me], gate_ss.at[d, e], gate_rs.at[d, e], at(to_q * S + to_s)
+        )
 
     def p_copy(d):
         return remote(tp_send.at[d], tp_recv.at[d], p_ss.at[d], p_rs.at[d], at(me, 1 - c))
 
-    def r_copy(d, e):
+    def r_copy(d, e, k):
         to = lax.rem(s + e, S)
-        return remote(tp_send.at[d, to], grp_recv.at[d, e], r_ss.at[d, e], r_rs.at[d, e], at(q * S + to))
-
-    def h_copy(d):
-        return remote(home_send.at[d], home_recv.at[q], h_ss.at[d], h_rs.at[d], at(source(d) * S + s))
-
-    def forward(d):
-        loop(1, S, lambda e: x_copy(d, e).start())
-        t_copy(d, 0).start()
-
-    for d in order[1:]:
-        z_copy(d).start()
-    forward(0)
+        part = pl.ds(k * RC, RC)
+        return remote(
+            tp_send.at[d, to, part], grp_recv.at[d, e, part], r_ss.at[d, e, k], r_rs.at[d, e, k], at(q * S + to)
+        )
+
+    def h_copy(d, k):
+        part = pl.ds(k * RC, RC)
+        return remote(
+            home_send.at[d, part], home_recv.at[q, part], h_ss.at[d, k], h_rs.at[d, k], at(source(d) * S + s)
+        )
+
+    def forward(d, k):
+        loop(1, S, lambda e: x_copy(d, e, k).start())
+        t_copy(d, 0, k).start()
+
+    for k in range(K):
+        forward(0, k)
+    for k in range(K):
+        z_copy(order[1], k).start()
 
     for g in range(Q):
         ids = g * group_width + lax.broadcasted_iota(jnp.int32, (gate_rows, tok), 0)
@@ -135,23 +156,33 @@
             precision=lax.Precision.HIGHEST, preferred_element_type=F32,
         )
     gate_recv[me] = gate_send[q]
-    loop(1, N, lambda p: gate_copy(p).start())
+
+    for d in order:
+        loop(1 if d == 0 else 0, S, lambda e: gate_copy(d, e).start())
+    for d in order[2:]:
+        for k in range(K):
+            z_copy(d, k).start()
+
     unpack[...] = jnp.concatenate([pick[:R] for pick in picks], axis=0).T.astype(BF16)
 
     def stage_a(d):
-        z_copy(d).wait_recv()
-        forward(d)
+        for k in range(K):
+            z_copy(d, k).wait_recv()
+            forward(d, k)
 
     def stage_b(d):
-        def one(e):
-            x_copy(d, e).wait_recv()
-            t_copy(d, e).start()
-        loop(1, S, one)
+        for k in range(K):
+            def one(e):
+                x_copy(d, e, k).wait_recv()
+                t_copy(d, e, k).start()
+            loop(1, S, one)
 
     pair = 2 if S % 2 == 0 else 1
 
     def stage_c(d):
-        loop(0, S, lambda e: t_copy(d, e).wait_recv())
+        loop(1 if d == 0 else 0, S, lambda e: gate_copy(d, e).wait_recv())
+        for k in range(K):
+            loop(0, S, lambda e: t_copy(d, e, k).wait_recv())
         src = source(d)
         diagonal = (
             lax.broadcasted_iota(jnp.int32, (R, lanes), 0) == lax.broadcasted_iota(jnp.int32, (R, lanes), 1)
@@ -180,7 +211,7 @@
             tp_send[d, pl.ds(base, pair)] = other.astype(BF16).reshape(pair, R, H)
             for j in range(L):
                 mine += jnp.dot(hidden[:, j * F:(j + 1) * F], w_down[j, :, own_cols], preferred_element_type=F32)
-            kept[pl.ds(base, pair)] = mine.reshape(pair, R, H)
+            kept[min(d, 1), pl.ds(base, pair)] = mine.reshape(pair, R, H)
 
         if S == pair:
             some(0)
@@ -190,61 +221,71 @@
 
     def stage_e(d):
         p_copy(d).wait()
-        def one(e):
-            to = lax.rem(s + e, S)
-            tp_send[d, to] = (kept[to] + tp_recv[d, to].astype(F32)).astype(BF16)
-            r_copy(d, e).start()
-        loop(1, S, one)
-        own_sum[...] = kept[s] + tp_recv[d, s].astype(F32)
+        for k in range(K):
+            part = pl.ds(k * RC, RC)
+
+            def one(e):
+                to = lax.rem(s + e, S)
+                tp_send[d, to, part] = (kept[min(d, 1), to, part] + tp_recv[d, to, part].astype(F32)).astype(BF16)
+                r_copy(d, e, k).start()
+            loop(1, S, one)
+        own_sum[d] = kept[min(d, 1), s] + tp_recv[d, s].astype(F32)
 
     def stage_f(d):
-        def one(e):
-            r_copy(d, e).wait_recv()
-            own_sum[...] += grp_recv[d, e].astype(F32)
-        loop(1, S, one)
-        if d == 0:
-            home_recv[q] = own_sum[...].astype(BF16)
-        else:
-            home_send[d] = own_sum[...].astype(BF16)
-            h_copy(d).start()
+        for k in range(K):
+            part = pl.ds(k * RC, RC)
+
+            def one(e):
+                r_copy(d, e, k).wait_recv()
+                own_sum[d, part] += grp_recv[d, e, part].astype(F32)
+            loop(1, S, one)
+            if d == 0:
+                home_recv[q, part] = own_sum[d, part].astype(BF16)
+            else:
+                home_send[d, part] = own_sum[d, part].astype(BF16)
+                h_copy(d, k).start()
 
     stage_b(0)
     for i in range(Q):
         if i + 1 < Q:
             stage_a(order[i + 1])
         if i == 0:
-            loop(1, N, lambda p: gate_copy(p).wait_recv())
             for copy in weights:
                 copy.wait()
-        if i >= 1:
-            if i >= 2:
-                stage_f(order[i - 2])
+        if i >= 3:
+            stage_f(order[i - 2])
+        if i >= 2:
             stage_e(order[i - 1])
         stage_c(order[i])
         if i + 1 < Q:
             stage_b(order[i + 1])
     if Q >= 2:
-        stage_f(order[Q - 2])
-    stage_e(order[Q - 1])
-    stage_f(order[Q - 1])
+        stage_e(order[Q - 1])
+    stage_e(0)
+    for d in order[max(1, Q - 2):]:
+        stage_f(d)
+    stage_f(0)
 
     for d in order[1:]:
-        h_copy(d).wait_recv()
+        for k in range(K):
+            h_copy(d, k).wait_recv()
     mixed = jnp.dot(unpack[...], home_recv[...].reshape(Q * R, H), preferred_element_type=F32)
     squares = jnp.sum(mixed * mixed, axis=1, keepdims=True)
     sq_send[...] = jnp.broadcast_to(squares, sq_send.shape)
     sq_copy = remote(sq_send, sq_recv, q_ss, q_rs, at(me, 1 - c))
     sq_copy.start()
-    for d in range(1, Q):
-        z_copy(d).wait_send()
-        h_copy(d).wait_send()
     for d in range(Q):
-        def sent(e):
-            x_copy(d, e).wait_send()
-            r_copy(d, e).wait_send()
-        loop(1, S, sent)
-        loop(0, S, lambda e: t_copy(d, e).wait_send())
-    loop(1, N, lambda p: gate_copy(p).wait_send())
+        loop(1 if d == 0 else 0, S, lambda e: gate_copy(d, e).wait_send())
+        for k in range(K):
+            if d > 0:
+                z_copy(d, k).wait_send()
+                h_copy(d, k).wait_send()
+
+            def sent(e):
+                x_copy(d, e, k).wait_send()
+                r_copy(d, e, k).wait_send()
+            loop(1, S, sent)
+            loop(0, S, lambda e: t_copy(d, e, k).wait_send())
     sq_copy.wait()
     total = squares + sq_recv[:, 0:1]
     out_ref[...] = (mixed * lax.rsqrt(total / width + EPS) * out_gain_ref[...]).astype(BF16)
@@ -269,9 +310,10 @@
     return pl.pallas_call(
         functools.partial(kernel, Q, S, R),
         out_shape=jax.ShapeDtypeStruct((tok, H), BF16),
-        in_specs=[vmem] * 5 + [hbm] * 3,
+        in_specs=[vmem] * 4 + [hbm] * 4,
         out_specs=vmem,
         scratch_shapes=[
+            pltpu.VMEM((tok, D), BF16),
             pltpu.VMEM((Q, R, H), BF16),
             pltpu.VMEM((Q, S, 2, R, H), BF16),
             pltpu.VMEM((tok, Q * R), BF16),
@@ -281,18 +323,18 @@
             pltpu.VMEM((L, D, F), BF16),
             pltpu.VMEM((L, F, D), BF16),
             pltpu.VMEM((pair * R, L * F), BF16),
-            pltpu.VMEM((S, R, H), F32),
+            pltpu.VMEM((2, S, R, H), F32),
             pltpu.VMEM((Q, S, R, H), BF16),
             pltpu.VMEM((Q, S, R, H), BF16),
-            pltpu.VMEM((R, H), F32),
+            pltpu.VMEM((Q, R, H), F32),
             pltpu.VMEM((Q, S, R, H), BF16),
             pltpu.VMEM((Q, R, H), BF16),
             pltpu.VMEM((Q, R, H), BF16),
             pltpu.VMEM((tok, 128), F32),
             pltpu.VMEM((tok, 128), F32),
-            dma((3, L)), dma((N,)), dma((N,)), dma((Q,)), dma((Q,)),
-            dma((Q, S)), dma((Q, S)), dma((Q, S)), dma((Q, S)),
-            dma((Q,)), dma((Q,)), dma((Q, S)), dma((Q, S)), dma((Q,)), dma((Q,)),
+            dma, dma((3, L)), dma((Q, S)), dma((Q, S)), dma((Q, CHUNKS)), dma((Q, CHUNKS)),
+            dma((Q, S, CHUNKS)), dma((Q, S, CHUNKS)), dma((Q, S, CHUNKS)), dma((Q, S, CHUNKS)),
+            dma((Q,)), dma((Q,)), dma((Q, S, CHUNKS)), dma((Q, S, CHUNKS)), dma((Q, CHUNKS)), dma((Q, CHUNKS)),
             dma, dma,
         ],
         compiler_params=pltpu.CompilerParams(

time: 52.4 us -> 47.5 us (0.906)
  Pallas kernels: 50.5 us -> 45.7 us
    pallas_call x1, Pallas kernels: 50.5 us -> 45.7 us  [body(): pl.pallas_call(functools.partial(kernel, Q, S, R), out_shape=jax.ShapeDty...]
where the time goes in v2:
time: 47.5 us; the launch traced here: 47.3 us
  Pallas kernels  45.7 us (96%)
  local copies, waits for them, and re-layouts  1.67 us (4%)
    pallas_call x1, Pallas kernels, body(): pl.pallas_call(functools.partial(kernel, Q, S, R), out_shape=jax.ShapeDty...  45.7 us
    unnamed x1, local copies, waits for them, and re-layouts  1.67 us

profile of v2, /device:TPU:0, one launch (start us, length us, event | category | flops | bytes accessed | tf_op | source)
XLA Modules:
  0.0 47.3 jit_solution(13923770184906444856)
XLA Ops:
  0.0 45.7 %shard_map.82 = bf16[128,1024]{1,0:T(8,128)(2,1)} custom-call(s32[4,128]{1,0:T(4,128)} %bitcast.6, f32[4,128]{1,0:T(4,128)} %bitcast.7, f32[1,2048]{1,0:T(1,128)} %bitcast.4, f32[1,1024]{1,0:T(1,128)} %bitcast.5, bf16[128,2048]{1,0:T(8,128)(2,1)} %tokens_hbm.1, bf16[2,2048,256]{2,1,0:T(8,128)(2,1)} %gate_hbm.1, bf16[2,2048,256]{2,1,0:T(8,128)(2,1)} %up_hbm.1, ...), custom_call_target="tpu_custom_call" | custom-call | tf_op jit(solution)/shard_map/pallas_call | solution.py:310
  45.7 1.7 %copy.10 = bf16[128,1024]{1,0:T(8,128)(2,1)} copy(bf16[128,1024]{1,0:T(8,128)(2,1)} %shard_map.82) | data formatting | bytes 524288
